TPU v7x, 512 devices: a whole 4x4x16 slice. The times are simulated.
512 devices in a mesh: sp: 64 (over z, y), tp: 8 (over x, core).
Axes of the slice: x: 4, y: 4, z: 16, core: 2. Of those that a mesh axis runs over, the one named last changes fastest.
Arguments:
- residual: bfloat16 [16384, 2048], P('sp'), may hold values from -6 to 6
- queries: bfloat16 [16384, 1024], P('sp', 'tp'), may hold values from -6 to 6
- forget_gate_logits: bfloat16 [16384, 1024], P('sp', 'tp'), may hold values from -5 to 5
- projected_values: bfloat16 [16384, 1024], P('sp', 'tp'), may hold values from -6 to 6
- output_gate_logits: bfloat16 [16384, 1024], P('sp', 'tp'), may hold values from -6 to 6
- lower_bound_margin: float32 [1024], P('tp'), may hold values from 6.1035156e-05 to 0.08
- extra_forget_logs: float32 [16384, 1024], P('sp', 'tp'), may hold values from -0.7 to 0
- per_head_norm_gain: float32 [128], replicated, may hold values from 0.1 to 1.9
- output_weight: bfloat16 [1024, 2048], P('tp'), may hold values from -0.1875 to 0.1875
- feedforward_norm_gain: float32 [2048], replicated, may hold values from 0.1 to 1.9
- gate_weight: bfloat16 [2048, 5632], P('sp', 'tp'), may hold values from -0.125 to 0.125
- up_weight: bfloat16 [2048, 5632], P('sp', 'tp'), may hold values from -0.125 to 0.125
- down_weight: bfloat16 [5632, 2048], P('tp', 'sp'), may hold values from -0.078125 to 0.078125
Outputs:
- layer_out: bfloat16 [16384, 2048], P('sp')
All inputs are finite; a program needn't handle non-finite values.
Results may differ from a plain program's by a relative error of at most 0.015.
Values may be sent and summed in bfloat16 or wider, within the bound.
No kernel may reach another device: no remote copies, remote signals or barrier semaphores. Data moves between devices by JAX's collectives and lax.ppermute only.
A program may use at most 64 MiB of HBM per device.

v0:
```python
import jax
import jax.numpy as jnp
from jax import lax
from jax.sharding import Mesh
from jax.sharding import PartitionSpec as P

HD = 128
BLOCK = 64
SP = ("sp_0", "sp_1")
eps = 1e-06


def gather_turned(arrays, axis, dims):
    turned = [jnp.moveaxis(a, dim, 0) for a, dim in zip(arrays, dims)]
    widths = [t[0].size for t in turned]
    both = jnp.concatenate([t.reshape(-1, w) for t, w in zip(turned, widths)], axis=1)
    filled = lax.all_gather(both, axis, axis=0, tiled=True)
    parts = jnp.split(filled, [sum(widths[:k]) for k in range(1, len(widths))], axis=1)
    return tuple(
        (
            jnp.moveaxis(b.reshape(-1, *t.shape[1:]), 0, dim)
            for b, t, dim in zip(parts, turned, dims)
        )
    )


def nothing_yet(value, identity):
    return jax.tree.map(
        lambda a, e: jnp.broadcast_to(jnp.asarray(e, a.dtype), a.shape), value, identity
    )


def gathered_once(value, axis):
    leaves = jax.tree.leaves(value)
    order = sorted(range(len(leaves)), key=lambda k: -leaves[k].size)
    width = (1, *leaves[order[0]].shape)[-1]
    lines = [
        jnp.pad(leaves[k].reshape(-1), (0, -leaves[k].size % width)).reshape(-1, width)
        for k in order
    ]
    both, at, found = (lax.all_gather(jnp.concatenate(lines), axis), 0, {})
    for k, line in zip(order, lines):
        section = both[:, at : at + len(line)].reshape(len(both), -1)
        found[k] = section[:, : leaves[k].size].reshape(-1, *leaves[k].shape)
        at += len(line)
    numbers = iter(range(len(leaves)))
    return jax.tree.map(lambda _: found[next(numbers)], value)


def carried_in_2(value, axes, combine, identity):
    before = start = nothing_yet(value, identity)
    running = value
    for axis in reversed(axes):
        length, place = (lax.axis_size(axis), lax.axis_index(axis))
        pieces = gathered_once(
            jax.tree.map(
                lambda part, kind: part.astype(kind), running, (jnp.bfloat16, jnp.bfloat16)
            ),
            axis,
        )
        inside, running = (start, start)
        for k in range(length):
            passed = k < place
            running = combine(
                running, jax.tree.map(lambda part, own: part[k].astype(own.dtype), pieces, value)
            )
            inside = jax.tree.map(lambda new, old: jnp.where(passed, new, old), running, inside)
        before = combine(inside, before)
    return before


def cut_along(value, dim, length):
    shape = value.shape
    parts = value.reshape(*shape[:dim], length, shape[dim] // length, *shape[dim + 1 :])
    return jnp.moveaxis(parts, dim, 0)


def sum_at_owner(value, axis, dim):
    parts = cut_along(value, dim, lax.axis_size(axis))
    arrived = lax.all_to_all(parts, axis, split_axis=0, concat_axis=0, tiled=True)
    return arrived.astype(jnp.float32).sum(axis=0)


def copy_for_each(value, axis):
    copies = jnp.broadcast_to(value, (lax.axis_size(axis), *value.shape))
    return lax.all_to_all(copies, axis, split_axis=0, concat_axis=0, tiled=True)


def laid_out(parts, dim):
    shape = list(parts.shape[1:])
    shape[dim] *= parts.shape[0]
    return jnp.moveaxis(parts, 0, dim).reshape(shape)


def collect(value, axis, dim):
    parts = copy_for_each(value, axis)
    return laid_out(parts, dim)


def block_update(carried_in, inputs):
    recurrent_state, offset = carried_in
    queries, state_increment, value_rows, retain_log_factor = inputs
    running_state = jnp.cumsum(retain_log_factor, axis=1)
    causal = jnp.tril(
        jnp.ones((retain_log_factor.shape[1], retain_log_factor.shape[1]), dtype=bool)
    )
    carried_over_state = jnp.einsum(
        "uqw,uwa->uqa", queries * jnp.exp(running_state), recurrent_state
    )
    spread = running_state[:, :, None, :] - running_state[:, None, :, :]
    weights = jnp.exp(jnp.where(causal[None, :, :, None], spread, -jnp.inf))
    scores = jnp.einsum("htk,htsk,hsk->hts", queries, weights, state_increment)
    output_rows = carried_over_state + jnp.einsum("hts,hsv->htv", scores, value_rows)
    final_state = running_state[:, -1:, :]
    updated_state = jnp.exp(final_state[:, 0, :])[:, :, None] * recurrent_state + jnp.einsum(
        "erb,erc->ebc", state_increment * jnp.exp(final_state - running_state), value_rows
    )
    rescaled_state = queries * jnp.exp(running_state + offset[:, None, :])
    return ((updated_state, offset + final_state[:, 0, :]), (output_rows, rescaled_state))


def join_states(earlier, later):
    earlier_sum, earlier_memory = earlier
    later_sum, later_memory = later
    return (earlier_sum + later_sum, jnp.exp(later_sum)[:, :, None] * earlier_memory + later_memory)


def local(
    residual,
    queries,
    forget_gate_logits,
    projected_values,
    output_gate_logits,
    lower_bound_margin,
    extra_forget_logs,
    per_head_norm_gain,
    output_weight,
    feedforward_norm_gain,
    gate_weight,
    up_weight,
    down_weight,
):
    gate_full, up_full, down_full = gather_turned(
        (gate_weight, up_weight, down_weight), SP, (0, 0, 1)
    )
    length = queries.shape[0]
    head_count = queries.shape[1] // HD
    state_increment = lower_bound_margin * jax.nn.sigmoid(-forget_gate_logits.astype(jnp.float32))
    retain_log_factor = jnp.log1p(-state_increment) + extra_forget_logs

    def to_blocks(source):
        return source.reshape(length // BLOCK, BLOCK, head_count, HD).transpose(0, 2, 1, 3)

    initial = (
        jnp.zeros((head_count, HD, HD), jnp.float32),
        jnp.zeros((head_count, HD), jnp.float32),
    )
    block_inputs = (
        to_blocks(queries.astype(jnp.float32)),
        to_blocks(state_increment),
        to_blocks(projected_values.astype(jnp.float32)),
        to_blocks(retain_log_factor),
    )
    (recurrent_state, decay_sum), (output_rows, rescaled_state) = lax.scan(
        block_update, initial, block_inputs
    )
    identity = (jnp.zeros_like(decay_sum), jnp.zeros_like(recurrent_state))
    incoming_state = carried_in_2((decay_sum, recurrent_state), SP, join_states, identity)[1]
    output_rows = output_rows + jnp.einsum("sjey,jyx->sjex", rescaled_state, incoming_state)
    mixed = output_rows.transpose(0, 2, 1, 3).reshape(length, head_count, HD)
    normed_heads = (
        mixed
        * lax.rsqrt(jnp.mean(mixed * mixed, axis=-1, keepdims=True) + eps)
        * per_head_norm_gain
    )
    gating = jax.nn.silu(output_gate_logits.astype(jnp.float32)).reshape(length, head_count, HD)
    gated = (normed_heads * gating).reshape(length, head_count * HD).astype(jnp.bfloat16)
    row_count = residual.shape[0] // lax.axis_size("tp")
    own_rows = lax.dynamic_slice_in_dim(residual, lax.axis_index("tp") * row_count, row_count, 0)
    rows_here = gated
    projected = sum_at_owner(
        jnp.dot(rows_here, output_weight, preferred_element_type=jnp.float32).astype(jnp.bfloat16),
        "tp",
        0,
    )
    after_mixer = (own_rows.astype(jnp.float32) + projected).astype(jnp.bfloat16)
    widened = after_mixer.astype(jnp.float32)
    normed = (
        widened
        * lax.rsqrt(jnp.mean(widened * widened, axis=-1, keepdims=True) + eps)
        * feedforward_norm_gain
    ).astype(jnp.bfloat16)
    row_piece = collect(normed, "tp", 0)
    gate_part = jnp.dot(row_piece, gate_full, preferred_element_type=jnp.float32)
    up_part = jnp.dot(row_piece, up_full, preferred_element_type=jnp.float32)
    hidden = (jax.nn.silu(gate_part) * up_part).astype(jnp.bfloat16)
    rows_here = hidden
    ffn_sum = sum_at_owner(
        jnp.dot(rows_here, down_full, preferred_element_type=jnp.float32).astype(jnp.bfloat16),
        "tp",
        0,
    )
    finished = (after_mixer.astype(jnp.float32) + 0.5 * ffn_sum).astype(jnp.bfloat16)
    return collect(finished, "tp", 0)


def solution(mesh):
    finer = Mesh(mesh.devices.reshape(16, 4, mesh.shape["tp"]), ("sp_0", "sp_1", "tp"))
    placed = (
        P(SP, None),
        P(SP, "tp"),
        P(SP, "tp"),
        P(SP, "tp"),
        P(SP, "tp"),
        P("tp"),
        P(SP, "tp"),
        P(),
        P("tp", None),
        P(),
        P(SP, "tp"),
        P(SP, "tp"),
        P("tp", SP),
    )
    return jax.shard_map(local, mesh=finer, in_specs=placed, out_specs=P(SP, None), check_vma=False)
```

profile of v0, /device:TPU:1, one launch (start us, length us, event | category | flops | bytes accessed | tf_op | source)
XLA Modules:
  0.0 229.9 jit_solution(110097667597470803)
XLA Ops:
  6.5 1.7 concatenate.11
  8.3 0.9 convert.7
  9.2 1.1 divide_multiply_fusion
  10.2 6.6 %while.17 = (s32[]{:T(128)}, f32[1,128,128]{2,1,0:T(8,128)S(1)}, f32[1,128]{1,0:T(1,128)S(1)}, f32[4,1,64,128]{3,2,1,0:T(8,128)S(1)}, bf16[4,1,64,128]{3,2,1,0:T...) while((s32[]{:T(128)}, f32[1,128,128]{2,1,0:T(8,128)S(1)}, ...), condition=%wide.region_2.3_spmd.clone, body=%wide.region_0.2_spmd.clone.sunk | while | flops 8499459 | bytes 1212596 | solution.py:164
  10.5 0.9 fusion.282
  11.4 0.1 fusion.281
  11.6 0.2 fusion.278
  12.1 0.9 fusion.282
  13.1 0.1 fusion.281
  13.2 0.2 fusion.278
  13.8 0.9 fusion.282
  14.7 0.1 fusion.281
  14.8 0.2 fusion.278
  15.4 0.9 fusion.282
  16.4 0.1 fusion.281
  16.5 0.2 fusion.278
  16.9 10.5 %all-gather.2 = bf16[4,129,128]{2,1,0:T(8,128)(2,1)S(1)} all-gather(bf16[1,129,128]{2,1,0:T(8,128)(2,1)S(1)} %maximum_bitcast_fusion), channel_id=2, replica_groups=mesh['sp_0'=16,'sp_1'=4,'tp'=8] {'sp_1'}, dimensions={0}, use_global_device_ids=true | all-gather | bytes 165120 | tf_op jit(solution)/shard_map/all_gather | solution.py:41
  27.5 33.0 %all-gather.3 = bf16[16,129,128]{2,1,0:T(8,128)(2,1)S(1)} all-gather(bf16[1,129,128]{2,1,0:T(8,128)(2,1)S(1)} %maximum_bitcast_fusion.1), channel_id=3, replica_groups=mesh['sp_0'=16,'sp_1'=4,'tp'=8] {'sp_0'}, dimensions={0}, use_global_device_ids=true | all-gather | bytes 561408 | tf_op jit(solution)/shard_map/all_gather | solution.py:41
  60.6 0.7 multiply_reduce_fusion
  61.5 1.4 convolution_convert_fusion
  62.9 14.1 %all-to-all-start = ((bf16[8,32,2048]{2,1,0:T(8,128)(2,1)}), bf16[8,32,2048]{2,1,0:T(8,128)(2,1)S(1)}, u32[]{:S(2)}, u32[]{:S(2)}) async-start(bf16[8,32,2048]{2,1,0:T(8,128)(2,1)} %bitcast.37), calls=%async_computation | async-start | bytes 2097152 | tf_op jit(solution)/shard_map/all_to_all | solution.py:80
  77.1 15.0 %all-to-all-done = bf16[8,32,2048]{2,1,0:T(8,128)(2,1)S(1)} async-done(((bf16[8,32,2048]{2,1,0:T(8,128)(2,1)}), bf16[8,32,2048]{2,1,0:T(8,128)(2,1)S(1)}, u32[]{:S(2)}, u32[]{:S(2)}) %all-to-all-start) | async-done | bytes 1048608 | tf_op jit(solution)/shard_map/all_to_all | solution.py:80
  92.0 0.1 convert_reduce_fusion.1
  92.2 1.1 fusion.65
  93.5 18.4 %all_to_all.20 = bf16[8,32,2048]{2,1,0:T(8,128)(2,1)S(1)} all-to-all(bf16[8,32,2048]{2,1,0:T(8,128)(2,1)S(1)} %broadcast_in_dim.28), channel_id=1, replica_groups=mesh['sp_0'=16,'sp_1'=4,'tp'=8] {'tp'}, dimensions={0} | all-to-all | bytes 2097152 | tf_op jit(solution)/shard_map/all_to_all | solution.py:86
  111.9 53.7 %all-gather.6.cloned.1.call-done = bf16[2048,2112]{1,0:T(8,128)(2,1)} async-done(((bf16[32,2112]{1,0:T(8,128)(2,1)}), bf16[2048,2112]{1,0:T(8,128)(2,1)}) %all-gather.6.cloned.1.call-update) | async-done | bytes 8650768 | tf_op jit(solution)/shard_map/all_gather | solution.py:17
  165.5 3.2 %fusion.45 = f32[256,704]{0,1:T(8,128)S(1)} fusion(bf16[256,2048]{1,0:T(8,128)(2,1)S(1)} %bitcast.209, bf16[2048,2112]{1,0:T(8,128)(2,1)} %all-gather.6.cloned.1.call-done), kind=kOutput, calls=%fused_computation.55 | convolution fusion | flops 738197504 | bytes 4915200 | tf_op jit(solution)/shard_map/dot_general | solution.py:194
  168.8 7.4 %fusion.47 = bf16[256,2048]{1,0:T(8,128)(2,1)S(1)} fusion(bf16[2048,2112]{1,0:T(8,128)(2,1)} %all-gather.6.cloned.1.call-done, bf16[256,2048]{1,0:T(8,128)(2,1)S(1)} %bitcast.210, f32[256,704]{0,1:T(8,128)S(1)} %fusion.45), kind=kOutput, calls=%fused_computation.58 | convolution fusion | flops 1478000640 | bytes 9109504 | tf_op jit(solution)/shard_map/dot_general | solution.py:199
  176.1 27.3 %all_to_all.21 = bf16[8,32,2048]{2,1,0:T(8,128)(2,1)S(1)} all-to-all(bf16[8,32,2048]{2,1,0:T(8,128)(2,1)S(1)} %bitcast.211), channel_id=1, replica_groups=mesh['sp_0'=16,'sp_1'=4,'tp'=8] {'tp'}, dimensions={0} | all-to-all | bytes 2097152 | tf_op jit(solution)/shard_map/all_to_all | solution.py:80
  203.4 0.1 convert_reduce_fusion
  203.7 18.4 %all_to_all.22 = bf16[8,32,2048]{2,1,0:T(8,128)(2,1)S(1)} all-to-all(bf16[8,32,2048]{2,1,0:T(8,128)(2,1)S(1)} %broadcast_in_dim.29), channel_id=1, replica_groups=mesh['sp_0'=16,'sp_1'=4,'tp'=8] {'tp'}, dimensions={0} | all-to-all | bytes 2097152 | tf_op jit(solution)/shard_map/all_to_all | solution.py:86
  222.1 1.0 copy.36
  (73 shorter events, 2.1 us)
Async XLA Ops:
  6.5 55.0 %copy-start = (bf16[128,2048]{1,0:T(8,128)(2,1)S(1)}, bf16[128,2048]{1,0:T(8,128)(2,1)}, u32[]{:S(2)}) copy-start(bf16[128,2048]{1,0:T(8,128)(2,1)} %param.23) | copy-start | bytes 1572868
  6.5 159.0 %all-gather.6.cloned.1.call-start = ((), (), s32[]{:S(2)}) async-start(), calls=%async_computation.4 | async-start | bytes 9052160 | tf_op jit(solution)/shard_map/all_gather | solution.py:17
  10.2 1.3 copy-start.1
  11.9 1.3 copy-start.1
  13.5 1.3 copy-start.1
  15.2 1.3 copy-start.1
  16.8 44.6 %copy-start.2 = (bf16[256,128]{1,0:T(8,128)(2,1)S(1)}, bf16[256,128]{1,0:T(8,128)(2,1)}, u32[]{:S(2)}) copy-start(bf16[256,128]{1,0:T(8,128)(2,1)} %param.19) | copy-start | bytes 196612
  16.8 44.6 %copy-start.4 = (f32[128]{0:T(128)S(1)}, f32[128]{0:T(128)}, u32[]{:S(2)}) copy-start(f32[128]{0:T(128)} %param.22) | copy-start | bytes 1540
  61.3 31.9 %copy-start.3 = (f32[2048]{0:T(1024)S(1)}, f32[2048]{0:T(1024)}, u32[]{:S(2)}) copy-start(f32[2048]{0:T(1024)} %param.24) | copy-start | bytes 24580
  62.9 29.1 %all-to-all-start = ((bf16[8,32,2048]{2,1,0:T(8,128)(2,1)}), bf16[8,32,2048]{2,1,0:T(8,128)(2,1)S(1)}, u32[]{:S(2)}, u32[]{:S(2)}) async-start(bf16[8,32,2048]{2,1,0:T(8,128)(2,1)} %bitcast.37), calls=%async_computation | async-start | bytes 2097152 | tf_op jit(solution)/shard_map/all_to_all | solution.py:80
Sparse Core Ops, SparseCore 0:
  10.3 155.2 all-gather.5
where the time goes:
time: 230 us
  blocking collectives  108 us (47%)
  waiting for transfers between devices  68.6 us (30%)
  matrix products  18.4 us (8%)
  starting transfers between devices  14.1 us (6%)
  between operations  13.6 us (6%)
  other arithmetic  4.28 us (2%)
  local copies, waits for them, and re-layouts  3.11 us (1%)
    all_gather x1, waiting for transfers between devices, gather_turned(): filled = lax.all_gather(both, axis, axis=0, tiled=True)  53.7 us
    all_gather x2, blocking collectives, gathered_once(): both, at, found = (lax.all_gather(jnp.concatenate(lines), axis), 0, {})  43.5 us
    all_to_all x2, blocking collectives, copy_for_each(): return lax.all_to_all(copies, axis, split_axis=0, concat_axis=0, tiled=True)  36.8 us
    all_to_all x1, blocking collectives, sum_at_owner(): lax.all_to_all(parts, axis, split_axis=0, concat_axis=0, tiled=True)  27.3 us
    all_to_all x1, waiting for transfers between devices, sum_at_owner(): lax.all_to_all(parts, axis, split_axis=0, concat_axis=0, tiled=True)  15 us
    all_to_all x1, starting transfers between devices, sum_at_owner(): lax.all_to_all(parts, axis, split_axis=0, concat_axis=0, tiled=True)  14.1 us
    dot_general x1, matrix products, local(): jnp.dot(rows_here, down_full, preferred_element_type=jnp.float32)  7.35 us
  transfers between devices with their start and end apart: 2, of which 2 were waited for; matrix products, arithmetic and copies ran while one was open for 5% of the time, Pallas kernels for 0%

commit v1 on v0

--- a/solution.py
+++ b/solution.py
@@ -14,7 +14,9 @@
     turned = [jnp.moveaxis(a, dim, 0) for a, dim in zip(arrays, dims)]
     widths = [t[0].size for t in turned]
     both = jnp.concatenate([t.reshape(-1, w) for t, w in zip(turned, widths)], axis=1)
-    filled = lax.all_gather(both, axis, axis=0, tiled=True)
+    filled = jnp.concatenate(
+        lax.all_to_all(jnp.stack([both] * lax.axis_size(axis)), axis, 0, 0), axis=0
+    )
     parts = jnp.split(filled, [sum(widths[:k]) for k in range(1, len(widths))], axis=1)
     return tuple(
         (

time: 230 us -> 564 us (2.45)
  blocking collectives: 108 us -> 480 us
  waiting for transfers between devices: 68.6 us -> 29.8 us
  between operations: 13.6 us -> 0.23 us
    all_to_all x0 -> x1, blocking collectives: none -> 398 us  [gather_turned(): lax.all_to_all(jnp.stack([both] * lax.axis_size(axis)), axis, 0, 0)]
    all_gather x1 -> x0, waiting for transfers between devices: 53.7 us -> none  [gather_turned(): filled = lax.all_gather(both, axis, axis=0, tiled=True)]
    all_to_all x2 -> x1, blocking collectives: 36.8 us -> 18.4 us  [copy_for_each(): return lax.all_to_all(copies, axis, split_axis=0, concat_axis=0, tiled=True)]
    all_to_all x0 -> x1, waiting for transfers between devices: none -> 14.9 us  [copy_for_each(): return lax.all_to_all(copies, axis, split_axis=0, concat_axis=0, tiled=True)]
    all_to_all x1, blocking collectives: 27.3 us -> 21.4 us  [sum_at_owner(): lax.all_to_all(parts, axis, split_axis=0, concat_axis=0, tiled=True)]
  transfers between devices with their start and end apart: 2 -> 2, of which waited for: 2 -> 2; matrix products, arithmetic and copies ran while one was open for 5% -> 0% of each run, Pallas kernels for 0% -> 0%
where the time goes in v1:
time: 564 us; the launch traced here: 563 us
  blocking collectives  480 us (85%)
  waiting for transfers between devices  29.8 us (5%)
  matrix products  22.2 us (4%)
  starting transfers between devices  19.1 us (3%)
  local copies, waits for them, and re-layouts  6.52 us (1%)
    all_to_all x1, blocking collectives, gather_turned(): lax.all_to_all(jnp.stack([both] * lax.axis_size(axis)), axis, 0, 0)  398 us
    all_gather x2, blocking collectives, gathered_once(): both, at, found = (lax.all_gather(jnp.concatenate(lines), axis), 0, {})  42 us
    all_to_all x1, blocking collectives, sum_at_owner(): lax.all_to_all(parts, axis, split_axis=0, concat_axis=0, tiled=True)  21.4 us
    all_to_all x1, blocking collectives, copy_for_each(): return lax.all_to_all(copies, axis, split_axis=0, concat_axis=0, tiled=True)  18.4 us
    all_to_all x1, waiting for transfers between devices, sum_at_owner(): lax.all_to_all(parts, axis, split_axis=0, concat_axis=0, tiled=True)  15 us
    all_to_all x1, waiting for transfers between devices, copy_for_each(): return lax.all_to_all(copies, axis, split_axis=0, concat_axis=0, tiled=True)  14.9 us
    all_to_all x1, starting transfers between devices, sum_at_owner(): lax.all_to_all(parts, axis, split_axis=0, concat_axis=0, tiled=True)  14.7 us
  transfers between devices with their start and end apart: 2, of which 2 were waited for; matrix products, arithmetic and copies ran while one was open for 0% of the time, Pallas kernels for 0%

profile of v1, /device:TPU:1, one launch (start us, length us, event | category | flops | bytes accessed | tf_op | source)
XLA Modules:
  0.0 562.5 jit_solution(12345478187086884484)
XLA Ops:
  0.0 0.9 convert.7
  0.9 1.1 divide_multiply_fusion
  2.0 12.2 %while.17 = (s32[]{:T(128)}, f32[1,128,128]{2,1,0:T(8,128)S(1)}, f32[1,128]{1,0:T(1,128)S(1)}, f32[4,1,64,128]{3,2,1,0:T(8,128)S(1)}, bf16[4,1,64,128]{3,2,1,0:T...) while((s32[]{:T(128)}, f32[1,128,128]{2,1,0:T(8,128)S(1)}, ...), condition=%wide.region_2.3_spmd.clone, body=%wide.region_0.2_spmd.clone.sunk | while | flops 8499459 | bytes 950424 | solution.py:166
  2.3 0.9 fusion.278
  3.3 0.9 fusion.282
  4.2 0.9 fusion.283
  5.4 0.9 fusion.278
  6.3 0.9 fusion.282
  7.3 0.9 fusion.283
  8.4 0.9 fusion.278
  9.4 0.9 fusion.282
  10.3 0.9 fusion.283
  11.5 0.9 fusion.278
  12.5 0.9 fusion.282
  13.4 0.9 fusion.283
  14.3 10.5 %all-gather.2 = bf16[4,129,128]{2,1,0:T(8,128)(2,1)S(1)} all-gather(bf16[1,129,128]{2,1,0:T(8,128)(2,1)S(1)} %maximum_bitcast_fusion), channel_id=2, replica_groups=mesh['sp_0'=16,'sp_1'=4,'tp'=8] {'sp_1'}, dimensions={0}, use_global_device_ids=true | all-gather | bytes 165120 | tf_op jit(solution)/shard_map/all_gather | solution.py:43
  24.9 31.6 %all-gather.3 = bf16[16,129,128]{2,1,0:T(8,128)(2,1)S(1)} all-gather(bf16[1,129,128]{2,1,0:T(8,128)(2,1)S(1)} %maximum_bitcast_fusion.1), channel_id=3, replica_groups=mesh['sp_0'=16,'sp_1'=4,'tp'=8] {'sp_0'}, dimensions={0}, use_global_device_ids=true | all-gather | bytes 561408 | tf_op jit(solution)/shard_map/all_gather | solution.py:43
  56.5 0.7 multiply_reduce_fusion
  57.5 1.4 convolution_convert_fusion
  58.9 14.7 %all-to-all-start = ((bf16[8,32,2048]{2,1,0:T(8,128)(2,1)}), bf16[8,32,2048]{2,1,0:T(8,128)(2,1)S(1)}, u32[]{:S(2)}, u32[]{:S(2)}) async-start(bf16[8,32,2048]{2,1,0:T(8,128)(2,1)} %bitcast.37), calls=%async_computation | async-start | bytes 2097152 | tf_op jit(solution)/shard_map/all_to_all | solution.py:82
  73.6 15.0 %all-to-all-done = bf16[8,32,2048]{2,1,0:T(8,128)(2,1)S(1)} async-done(((bf16[8,32,2048]{2,1,0:T(8,128)(2,1)}), bf16[8,32,2048]{2,1,0:T(8,128)(2,1)S(1)}, u32[]{:S(2)}, u32[]{:S(2)}) %all-to-all-start) | async-done | bytes 1048608 | tf_op jit(solution)/shard_map/all_to_all | solution.py:82
  88.7 1.1 fusion.65
  89.9 1.1 broadcast_in_dim.28
  91.0 4.4 all-to-all-start.1
  95.5 14.9 %all-to-all-done.1 = bf16[8,32,2048]{2,1,0:T(8,128)(2,1)S(1)} async-done(((bf16[8,32,2048]{2,1,0:T(8,128)(2,1)}), bf16[8,32,2048]{2,1,0:T(8,128)(2,1)S(1)}, u32[]{:S(2)}, u32[]{:S(2)}) %all-to-all-start.1) | async-done | bytes 1048608 | tf_op jit(solution)/shard_map/all_to_all | solution.py:88
  111.0 398.3 %all_to_all.25 = bf16[64,32,2112]{2,1,0:T(8,128)(2,1)S(1)} all-to-all(bf16[64,32,2112]{2,1,0:T(8,128)(2,1)S(1)} %stack.2), channel_id=1, replica_groups=mesh['sp_0'=16,'sp_1'=4,'tp'=8] {'sp_0','sp_1'}, dimensions={0} | all-to-all | bytes 17301504 | tf_op jit(solution)/shard_map/all_to_all | solution.py:18
  509.3 3.4 copy-done.1
  512.7 1.3 fusion.45
  514.1 7.3 %fusion.47 = bf16[256,2048]{1,0:T(8,128)(2,1)S(1)} fusion(bf16[2048,2112]{1,0:T(8,128)(2,1)} %bitcast.208, bf16[256,2048]{1,0:T(8,128)(2,1)S(1)} %bitcast.213, f32[256,704]{0,1:T(8,128)S(1)} %fusion.45), kind=kOutput, calls=%fused_computation.58 | convolution fusion | flops 1478000640 | bytes 9109504 | tf_op jit(solution)/shard_map/dot_general | solution.py:201
  521.4 21.4 %all_to_all.26 = bf16[8,32,2048]{2,1,0:T(8,128)(2,1)S(1)} all-to-all(bf16[8,32,2048]{2,1,0:T(8,128)(2,1)S(1)} %bitcast.214), channel_id=1, replica_groups=mesh['sp_0'=16,'sp_1'=4,'tp'=8] {'tp'}, dimensions={0} | all-to-all | bytes 2097152 | tf_op jit(solution)/shard_map/all_to_all | solution.py:82
  543.1 18.4 %all_to_all.27 = bf16[8,32,2048]{2,1,0:T(8,128)(2,1)S(1)} all-to-all(bf16[8,32,2048]{2,1,0:T(8,128)(2,1)S(1)} %broadcast_in_dim.29), channel_id=1, replica_groups=mesh['sp_0'=16,'sp_1'=4,'tp'=8] {'tp'}, dimensions={0} | all-to-all | bytes 2097152 | tf_op jit(solution)/shard_map/all_to_all | solution.py:88
  561.5 1.0 copy.36
  (73 shorter events, 2.9 us)
Async XLA Ops:
  0.0 57.5 %copy-start = (bf16[128,2048]{1,0:T(8,128)(2,1)S(1)}, bf16[128,2048]{1,0:T(8,128)(2,1)}, u32[]{:S(2)}) copy-start(bf16[128,2048]{1,0:T(8,128)(2,1)} %param.23) | copy-start | bytes 1572868
  14.2 43.1 %copy-start.2 = (bf16[256,128]{1,0:T(8,128)(2,1)S(1)}, bf16[256,128]{1,0:T(8,128)(2,1)}, u32[]{:S(2)}) copy-start(bf16[256,128]{1,0:T(8,128)(2,1)} %param.19) | copy-start | bytes 196612
  14.2 43.1 %copy-start.7 = (f32[128]{0:T(128)S(1)}, f32[128]{0:T(128)}, u32[]{:S(2)}) copy-start(f32[128]{0:T(128)} %param.22) | copy-start | bytes 1540
  57.2 32.5 %copy-start.6 = (f32[2048]{0:T(1024)S(1)}, f32[2048]{0:T(1024)}, u32[]{:S(2)}) copy-start(f32[2048]{0:T(1024)} %param.24) | copy-start | bytes 24580
  58.9 29.7 %all-to-all-start = ((bf16[8,32,2048]{2,1,0:T(8,128)(2,1)}), bf16[8,32,2048]{2,1,0:T(8,128)(2,1)S(1)}, u32[]{:S(2)}, u32[]{:S(2)}) async-start(bf16[8,32,2048]{2,1,0:T(8,128)(2,1)} %bitcast.37), calls=%async_computation | async-start | bytes 2097152 | tf_op jit(solution)/shard_map/all_to_all | solution.py:82
  73.6 21.8 %copy-start.3 = (bf16[32,704]{1,0:T(8,128)(2,1)S(1)}, bf16[32,704]{1,0:T(8,128)(2,1)}, u32[]{:S(2)}) copy-start(bf16[32,704]{1,0:T(8,128)(2,1)} %param.25) | copy-start | bytes 135172
  73.6 21.8 %copy-start.4 = (bf16[32,704]{1,0:T(8,128)(2,1)S(1)}, bf16[32,704]{1,0:T(8,128)(2,1)}, u32[]{:S(2)}) copy-start(bf16[32,704]{1,0:T(8,128)(2,1)} %param.26) | copy-start | bytes 135172
  73.6 21.8 %copy-start.5 = (bf16[704,32]{0,1:T(8,128)(2,1)S(1)}, bf16[704,32]{0,1:T(8,128)(2,1)}, u32[]{:S(2)}) copy-start(bf16[704,32]{0,1:T(8,128)(2,1)} %param.27) | copy-start | bytes 135172
  91.0 19.4 %all-to-all-start.1 = ((bf16[8,32,2048]{2,1,0:T(8,128)(2,1)}), bf16[8,32,2048]{2,1,0:T(8,128)(2,1)S(1)}, u32[]{:S(2)}, u32[]{:S(2)}) async-start(bf16[8,32,2048]{2,1,0:T(8,128)(2,1)} %broadcast_in_dim.28), calls=%async_computation.1 | async-start | bytes 2097152 | tf_op jit(solution)/shard_map/all_to_all | solution.py:88
  509.3 3.4 copy-start.1
